TPU v7x, 32 devices: a whole 2x2x4 slice. The times are simulated.
32 devices in a mesh: fs: 16 (over z, y, x), tp: 2 (over core).
Axes of the slice: x: 2, y: 2, z: 4, core: 2. Of those that a mesh axis runs over, the one named last changes fastest.
Arguments:
- late_input: bfloat16 [2048, 2048], P('fs', 'tp'), may hold values from -6 to 6
- up_weight: bfloat16 [2048, 4096], P('tp', 'fs'), may hold values from -0.125 to 0.125
- down_weight: bfloat16 [4096, 2048], P('fs', 'tp'), may hold values from -0.09375 to 0.09375
- early_input: bfloat16 [2048, 2048], P('fs', 'tp'), may hold values from -6 to 6
- early_pre: bfloat16 [2048, 4096], P('fs'), may hold values from -6 to 6
- cotangent: bfloat16 [2048, 2048], P('fs', 'tp'), may hold values from -6 to 6
- up_sum: float32 [2048, 4096], P('tp', 'fs'), may hold values from -24 to 24
- down_sum: float32 [4096, 2048], P('fs', 'tp'), may hold values from -24 to 24
Outputs:
- late_pre: bfloat16 [2048, 4096], P('fs')
- late_out: bfloat16 [2048, 2048], P('fs', 'tp')
- input_grad: bfloat16 [2048, 2048], P('fs', 'tp')
- up_total: float32 [2048, 4096], P('tp', 'fs')
- down_total: float32 [4096, 2048], P('fs', 'tp')
All inputs are finite; a program needn't handle non-finite values.
Results may differ from a plain program's by a relative error of at most 0.025.
Values may be sent and summed in bfloat16 or wider, within the bound.
A program may use at most 128 MiB of HBM per device.

v0:
```python
import jax
import jax.numpy as jnp
from jax import lax
from jax.experimental import pallas as pl
from jax.experimental.pallas import tpu as pltpu
from jax.sharding import PartitionSpec as P

MESH = pl.DeviceIdType.MESH
F32 = jnp.float32
BF16 = jnp.bfloat16


def dot(left, right, lc, rc):
    return lax.dot_general(left, right, (((lc,), (rc,)), ((), ())), preferred_element_type=F32)


def square_relu(value):
    kept = jnp.maximum(value.astype(F32), 0.0)
    return (kept * kept).astype(BF16)


def fused(a, late_in, up_w, down_w, early_in, early_pre, cot,
          late_pre_o, late_out_o, in_grad_o, up_o, down_o,
          cot_g, late_g, early_g, pre_g, up_g, down_g, gt_s, gt_r, pg, eh, lt_s, lt_r, lp, lh, lp_g,
          part, ig_s, ig_u, ig_d, lo_s, lo_u, lo_d,
          dg_s, dg_x, dg_y, dg_fx, dg_fy, ug_s, ug_x, ug_y, ug_fx, ug_fy,
          ag_ss, ag_rs, w_ss, w_rs, e_ss, e_rs, l_ss, l_rs, t_ss, t_rs, rl_ss, rl_rs, rq_ss, rq_rs,
          local_s, down_v, up_v, ig_v, lo_v):
    side = 4
    half_side = side // 2
    me = lax.axis_index("fs")
    t = lax.axis_index("tp")
    z = me // side
    q = lax.rem(me, side)
    y = q // 2
    x = lax.rem(q, 2)
    qx = y * 2 + (1 - x)
    qy = (1 - y) * 2 + x
    qd = side - 1 - q
    xn = (z * side + qx, t)
    yn = (z * side + qy, t)
    pn = (me, 1 - t)
    above = (lax.rem(me + side, a * side), t)
    below = (lax.rem(me + (a - 1) * side, a * side), t)
    rows = late_in.shape[0]
    ff = up_w.shape[1]
    width = late_in.shape[1]
    cols = ff * side
    step_n = width // side

    def begin(src, dst, k):
        copy = pltpu.make_async_copy(src, dst, local_s.at[k])
        copy.start()
        return copy

    own_rows = pl.ds(pl.multiple_of(z * rows, rows), rows)
    own_down = begin(down_w, down_g.at[q], 0)
    own_cot = begin(cot, cot_g.at[own_rows], 1)
    own_up = begin(up_w, up_g.at[q], 2)
    own_late = begin(late_in, late_g.at[own_rows], 3)
    own_early = begin(early_in, early_g.at[own_rows], 4)
    own_pre = [
        begin(early_pre.at[:, pl.ds(pl.multiple_of((z * side + b) * ff, ff), ff)],
              pre_g.at[b, own_rows], 5 + b)
        for b in range(side)
    ]

    barrier = pltpu.get_barrier_semaphore()
    greet = [xn, yn, pn] + [(lax.rem(me + o * side, a * side), t) for o in range(1, a)]
    for device in greet:
        pl.semaphore_signal(barrier, inc=1, device_id=device, device_id_type=MESH)
    pl.semaphore_wait(barrier, len(greet))

    sent = []

    def rc(src, dst, ss, rs, device):
        return pltpu.make_async_remote_copy(
            src_ref=src, dst_ref=dst, send_sem=ss, recv_sem=rs, device_id=device, device_id_type=MESH)

    def send(src, dst, ss, rs, device, cond=None):
        def go():
            rc(src, dst, ss, rs, device).start()

        if cond is None:
            go()
        else:
            pl.when(cond)(go)
        sent.append((cond, rc(src, dst, ss, rs, device)))

    def arrive(dst, ss, rs, cond=None):
        def go():
            rc(dst, dst, ss, rs, pn).wait_recv()

        if cond is None:
            go()
        else:
            pl.when(cond)(go)

    def slot(j):
        return pl.ds(pl.multiple_of(j * rows, rows), rows)

    def line_gather(which, own, buf, d):
        for way in range(2):
            if way == 0:
                j, here, on, device = z - d, z >= d, (z >= d) & (z < a - 1), above
            else:
                j, here, on, device = z + d, z + d < a, (z + d < a) & (z > 0), below
            j = jnp.clip(j, 0, a - 1)
            place = buf.at[slot(j)]
            if d > 0:
                arrive(place, ag_ss.at[which, way, 0], ag_rs.at[which, way, d], here)
            if d < a - 1:
                send(own if d == 0 else place, place, ag_ss.at[which, way, d],
                     ag_rs.at[which, way, d + 1], device, on)

    def half(ref, block, h):
        n = ref.shape[1] // 2
        return ref.at[block, pl.ds(h * n, n)]

    def half2(ref, h):
        n = ref.shape[0] // 2
        return ref.at[pl.ds(h * n, n)]

    def square_send(which, own, buf):
        for h in (0, 1):
            send(half2(own, h), half(buf, q, h), w_ss.at[which, 0, h], w_rs.at[which, 0, h], xn)
            send(half2(own, 1 - h), half(buf, q, 1 - h), w_ss.at[which, 1, 1 - h], w_rs.at[which, 1, 1 - h], yn)

    def square_relay(which, buf):
        arrive(half(buf, qx, 0), w_ss.at[which, 0, 0], w_rs.at[which, 0, 0])
        send(half(buf, qx, 0), half(buf, qx, 0), w_ss.at[which, 1, 2], w_rs.at[which, 1, 2], yn)
        arrive(half(buf, qy, 1), w_ss.at[which, 0, 0], w_rs.at[which, 1, 1])
        send(half(buf, qy, 1), half(buf, qy, 1), w_ss.at[which, 0, 2], w_rs.at[which, 0, 2], xn)

    def square_rest(which, buf):
        arrive(half(buf, qx, 1), w_ss.at[which, 0, 0], w_rs.at[which, 0, 1])
        arrive(half(buf, qy, 0), w_ss.at[which, 0, 0], w_rs.at[which, 1, 0])
        arrive(half(buf, qd, 0), w_ss.at[which, 0, 0], w_rs.at[which, 1, 2])
        arrive(half(buf, qd, 1), w_ss.at[which, 0, 0], w_rs.at[which, 0, 2])

    def square_sum_begin(which, block, staged, first_x, first_y, fin_x, fin_y):
        staged[qd] = block(qd).astype(BF16)
        send(half(staged, qd, 0), first_x, rq_ss.at[which, 0], rq_rs.at[which, 0], xn)
        send(half(staged, qd, 1), first_y, rq_ss.at[which, 1], rq_rs.at[which, 1], yn)
        staged[qx] = block(qx).astype(BF16)
        send(half(staged, qx, 0), half2(fin_x, 0), rq_ss.at[which, 2], rq_rs.at[which, 2], xn)
        staged[qy] = block(qy).astype(BF16)
        send(half(staged, qy, 1), half2(fin_y, 1), rq_ss.at[which, 3], rq_rs.at[which, 3], yn)

    def square_sum_relay(which, staged, first_x, first_y, fin_x, fin_y):
        n = staged.shape[1] // 2
        arrive(first_x, rq_ss.at[which, 0], rq_rs.at[which, 0])
        staged[qy, 0:n] = (staged[qy, 0:n].astype(F32) + first_x[...].astype(F32)).astype(BF16)
        send(half(staged, qy, 0), half2(fin_y, 0), rq_ss.at[which, 4], rq_rs.at[which, 4], yn)
        arrive(first_y, rq_ss.at[which, 0], rq_rs.at[which, 1])
        staged[qx, n:2 * n] = (staged[qx, n:2 * n].astype(F32) + first_y[...].astype(F32)).astype(BF16)
        send(half(staged, qx, 1), half2(fin_x, 1), rq_ss.at[which, 5], rq_rs.at[which, 5], xn)

    def square_sum_end(which, fin_x, fin_y, out):
        arrive(half2(fin_x, 0), rq_ss.at[which, 0], rq_rs.at[which, 2])
        arrive(half2(fin_y, 1), rq_ss.at[which, 0], rq_rs.at[which, 3])
        arrive(half2(fin_y, 0), rq_ss.at[which, 0], rq_rs.at[which, 4])
        arrive(half2(fin_x, 1), rq_ss.at[which, 0], rq_rs.at[which, 5])
        out[...] = out[...] + (fin_x[...].astype(F32) + fin_y[...].astype(F32))

    def line_sum_step(which, staged, from_u, from_d, step):
        for way in range(2):
            if way == 0:
                j, on, more, buf, device = a - 1 + z - step, step >= z, z > 0, from_u, above
            else:
                j, on, more, buf, device = step - (a - 1 - z), step >= a - 1 - z, z < a - 1, from_d, below
            j = jnp.clip(j, 0, a - 1)

            @pl.when(on & more)
            def _(j=j, buf=buf, way=way):
                arrive(buf.at[j], rl_ss.at[which, 0, 0], rl_rs.at[which, way, j])
                staged[j] = (staged[j].astype(F32) + buf[j].astype(F32)).astype(BF16)

            send(staged.at[j], buf.at[j], rl_ss.at[which, way, step], rl_rs.at[which, way, j], device, on)

    def line_sum_end(which, own, from_u, from_d, out):
        @pl.when(z > 0)
        def _():
            arrive(from_u.at[z], rl_ss.at[which, 0, 0], rl_rs.at[which, 0, z])
            own[slot(z)] = own[slot(z)] + from_u[z].astype(F32)

        @pl.when(z < a - 1)
        def _():
            arrive(from_d.at[z], rl_ss.at[which, 0, 0], rl_rs.at[which, 1, z])
            own[slot(z)] = own[slot(z)] + from_d[z].astype(F32)

        out[...] = own[slot(z)].astype(BF16)

    def columns(block, unit):
        return pl.ds(pl.multiple_of(block * unit, unit), unit)

    def hops(b_of, go):
        for o in range(1, a):
            zs = lax.rem(z - o + a, a)
            for u in range(half_side):
                go(o, u, zs, b_of(u))

    mine = lambda u: t * half_side + u
    other = lambda u: (1 - t) * half_side + u

    def to_line(which, value, staged):
        @pl.loop(0, side)
        def _(n):
            at = columns(n, step_n)
            part[which, :, at] = value(at)

        for j in range(a):
            staged[j] = part[which, pl.ds(j * rows, rows)].astype(BF16)

    def pre_relay(o, u, zs, b):
        place = pre_g.at[b, slot(zs)]
        arrive(place, e_ss.at[0, 0, 0], e_rs.at[0, o, u])
        send(place, place, e_ss.at[1, o, u], e_rs.at[1, o, u], pn)

    def pre_rest(o, u, zs, b):
        arrive(pre_g.at[b, slot(zs)], e_ss.at[0, 0, 0], e_rs.at[1, o, u])

    def out_relay(o, u, zs, b):
        place = lp_g.at[:, columns(zs * side + b, ff)]
        arrive(place, l_ss.at[0, 0, 0], l_rs.at[0, o, u])
        send(place, place, l_ss.at[1, o, u], l_rs.at[1, o, u], pn)

    def out_rest(o, u, zs, b):
        arrive(lp_g.at[:, columns(zs * side + b, ff)], l_ss.at[0, 0, 0], l_rs.at[1, o, u])

    def gather_late(d):
        if d < a:
            line_gather(1, late_g.at[slot(z)], late_g, d)

    def gather_early(d):
        if d < a:
            line_gather(2, early_g.at[slot(z)], early_g, d)

    def gather_cot(d):
        if d < a:
            line_gather(0, cot_g.at[slot(z)], cot_g, d)

    def sum_ig(k):
        if k < a:
            line_sum_step(0, ig_s, ig_u, ig_d, k - 1)

    def sum_lo(k):
        if k < a:
            line_sum_step(1, lo_s, lo_u, lo_d, k - 1)

    own_down.wait()
    square_send(1, down_g.at[q], down_g)
    own_cot.wait()
    gather_cot(0)
    for o in range(1, a):
        zd = lax.rem(z + o, a)
        for u in range(half_side):
            b = mine(u)
            send(early_pre.at[:, columns(zd * side + b, ff)], pre_g.at[b, slot(z)],
                 e_ss.at[0, o, u], e_rs.at[0, o, u], (zd * side + q, t))
    for copy in own_pre:
        copy.wait()
    gather_cot(1)
    square_relay(1, down_g)
    own_up.wait()
    square_send(0, up_g.at[q], up_g)
    own_late.wait()
    gather_late(0)
    gather_cot(2)
    hops(mine, pre_relay)
    for d in range(3, a):
        gather_cot(d)
    square_rest(1, down_g)
    gather_late(1)
    square_relay(0, up_g)

    @pl.loop(0, side)
    def _(b):
        gt_s[b] = dot(cot_g[...], down_g[b], 1, 1).astype(BF16)

    send(gt_s, gt_r, t_ss.at[0], t_rs.at[0], pn)
    own_early.wait()
    gather_early(0)
    hops(other, pre_rest)

    @pl.loop(0, side)
    def _(b):
        eh[b] = square_relu(pre_g[b])

    square_sum_begin(1, lambda b: dot(eh[b], cot_g[...], 0, 0), dg_s, dg_x, dg_y, dg_fx, dg_fy)
    arrive(gt_r, t_ss.at[0], t_rs.at[0])

    @pl.loop(0, side)
    def _(b):
        hidden = gt_s[b].astype(F32) + gt_r[b].astype(F32)
        pg[b] = (hidden * 2.0 * jnp.maximum(pre_g[b].astype(F32), 0.0)).astype(BF16)

    gather_late(2)
    square_rest(0, up_g)

    def ig_value(at):
        return sum(dot(pg[b], up_g[b, at, :], 1, 1) for b in range(side))

    to_line(0, ig_value, ig_s)
    sum_ig(1)
    for d in range(3, a):
        gather_late(d)

    @pl.loop(0, side)
    def _(b):
        lt_s[b] = dot(late_g[...], up_g[b], 1, 0).astype(BF16)

    send(lt_s, lt_r, t_ss.at[1], t_rs.at[1], pn)
    sum_ig(2)
    gather_early(1)
    square_sum_relay(1, dg_s, dg_x, dg_y, dg_fx, dg_fy)
    arrive(lt_r, t_ss.at[1], t_rs.at[1])

    @pl.loop(0, side)
    def _(b):
        pre = (lt_s[b].astype(F32) + lt_r[b].astype(F32)).astype(BF16)
        lp[b] = pre
        lh[b] = square_relu(pre)

    for o in range(1, a):
        zd = lax.rem(z + o, a)
        for u in range(half_side):
            b = mine(u)
            send(lp.at[b, slot(zd)], lp_g.at[:, columns(z * side + b, ff)],
                 l_ss.at[0, o, u], l_rs.at[0, o, u], (zd * side + q, t))
    for b in range(side):
        lp_g[:, columns(z * side + b, ff)] = lp[b, slot(z)]

    def lo_value(at):
        return sum(dot(lh[b], down_g[b, :, at], 1, 0) for b in range(side))

    to_line(1, lo_value, lo_s)
    sum_lo(1)
    gather_early(2)
    for k in range(3, a):
        sum_ig(k)
    sum_lo(2)
    down_v[...] = dot(eh[q], cot_g[...], 0, 0)
    for d in range(3, a):
        gather_early(d)
    square_sum_begin(0, lambda b: dot(early_g[...], pg[b], 0, 0), ug_s, ug_x, ug_y, ug_fx, ug_fy)
    up_v[...] = dot(early_g[...], pg[q], 0, 0)
    hops(mine, out_relay)
    square_sum_end(1, dg_fx, dg_fy, down_v)
    out_down = begin(down_v, down_o, 9)
    for k in range(3, a):
        sum_lo(k)
    line_sum_end(0, part.at[0], ig_u, ig_d, ig_v)
    out_ig = begin(ig_v, in_grad_o, 10)
    square_sum_relay(0, ug_s, ug_x, ug_y, ug_fx, ug_fy)
    hops(other, out_rest)
    out_pre = begin(lp_g, late_pre_o, 11)
    line_sum_end(1, part.at[1], lo_u, lo_d, lo_v)
    out_lo = begin(lo_v, late_out_o, 12)
    square_sum_end(0, ug_fx, ug_fy, up_v)
    out_up = begin(up_v, up_o, 13)

    for cond, copy in sent:
        if cond is None:
            copy.wait_send()
        else:
            pl.when(cond)(copy.wait_send)
    for copy in (out_down, out_ig, out_pre, out_lo, out_up):
        copy.wait()


def fused_body(late_input, up_weight, down_weight, early_input, early_pre, cotangent, up_sum, down_sum):
    a = lax.axis_size("fs") // 4
    side = 4
    rows, width = late_input.shape
    ff = up_weight.shape[1]
    tokens, hidden = rows * a, ff * side
    V = pltpu.VMEM
    D = pltpu.SemaphoreType.DMA
    token_block = V((tokens, width), BF16)
    hidden_block = V((side, tokens, ff), BF16)
    line_block = V((a, rows, width), BF16)
    scratch = (
        [token_block] * 3
        + [hidden_block, V((side, width, ff), BF16), V((side, ff, width), BF16)]
        + [hidden_block] * 8
        + [V((rows, hidden * a), BF16), V((2, tokens, width), F32)]
        + [line_block] * 6
        + [V((side, ff, width), BF16)] + [V((ff // 2, width), BF16)] * 2 + [V((ff, width), BF16)] * 2
        + [V((side, width, ff), BF16)] + [V((width // 2, ff), BF16)] * 2 + [V((width, ff), BF16)] * 2
        + [D((3, 2, a)), D((3, 2, a)), D((2, 2, 3)), D((2, 2, 3)), D((2, a, 2)), D((2, a, 2)),
           D((2, a, 2)), D((2, a, 2)), D((2,)), D((2,)), D((2, 2, a)), D((2, 2, a)), D((2, 6)), D((2, 6)), D((14,))]
        + [V((ff, width), F32), V((width, ff), F32)] + [V((rows, width), BF16)] * 2
    )
    flops = 12 * tokens * hidden * width
    late_pre, late_out, input_grad, up_grad, down_grad = pl.pallas_call(
        lambda *refs: fused(a, *refs),
        out_shape=(
            jax.ShapeDtypeStruct(early_pre.shape, BF16),
            jax.ShapeDtypeStruct(late_input.shape, BF16),
            jax.ShapeDtypeStruct(early_input.shape, BF16),
            jax.ShapeDtypeStruct(up_sum.shape, F32),
            jax.ShapeDtypeStruct(down_sum.shape, F32),
        ),
        in_specs=[pl.BlockSpec(memory_space=pl.ANY)] * 6,
        out_specs=[pl.BlockSpec(memory_space=pl.ANY)] * 5,
        scratch_shapes=scratch,
        compiler_params=pltpu.CompilerParams(
            collective_id=0, has_side_effects=True, vmem_limit_bytes=62 * 1024 * 1024),
        cost_estimate=pl.CostEstimate(flops=flops, bytes_accessed=1 << 24, transcendentals=0),
    )(late_input, up_weight, down_weight, early_input, early_pre, cotangent)
    return late_pre, late_out, input_grad, up_sum + up_grad, down_sum + down_grad


def contract_rows(left, right):
    return lax.dot_general(
        left, right, (((0,), (0,)), ((), ())), preferred_element_type=jnp.float32
    )


def contract_cols(left, right):
    return lax.dot_general(
        left, right, (((1,), (1,)), ((), ())), preferred_element_type=jnp.float32
    )


def body(late_input, up_weight, down_weight, early_input, early_pre, cotangent, up_sum, down_sum):
    up_gathered = lax.all_gather(up_weight, "fs", axis=1, tiled=True)
    down_gathered = lax.all_gather(down_weight, "fs", axis=0, tiled=True)
    pre_terms = jnp.dot(late_input, up_gathered, preferred_element_type=jnp.float32)
    pre_summed = lax.psum(pre_terms.astype(jnp.bfloat16), "tp")
    late_hidden = jnp.square(jax.nn.relu(pre_summed.astype(jnp.float32))).astype(jnp.bfloat16)
    early_float = early_pre.astype(jnp.float32)
    early_hidden = jnp.square(jax.nn.relu(early_float)).astype(jnp.bfloat16)
    late_out = jnp.dot(late_hidden, down_gathered, preferred_element_type=jnp.float32).astype(
        jnp.bfloat16
    )
    grad_terms = contract_cols(cotangent, down_gathered)
    hidden_grad = lax.psum(grad_terms.astype(jnp.bfloat16), "tp").astype(jnp.float32)
    pre_grad = (hidden_grad * 2.0 * jax.nn.relu(early_float)).astype(jnp.bfloat16)
    input_grad = contract_cols(pre_grad, up_gathered).astype(jnp.bfloat16)
    grad_local, hidden_local = (
        lax.all_to_all(pre_grad, "fs", split_axis=1, concat_axis=0, tiled=True),
        lax.all_to_all(early_hidden, "fs", split_axis=1, concat_axis=0, tiled=True),
    )
    rows = grad_local
    up_grad = contract_rows(lax.all_gather(early_input, "fs", axis=0, tiled=True), rows)
    up_total = up_sum + up_grad
    rows = hidden_local
    down_grad = contract_rows(rows, lax.all_gather(cotangent, "fs", axis=0, tiled=True))
    down_total = down_sum + down_grad
    return (pre_summed, late_out, input_grad, up_total, down_total)


def solution(mesh):
    in_specs = (
        P("fs", "tp"),
        P("tp", "fs"),
        P("fs", "tp"),
        P("fs", "tp"),
        P("fs", None),
        P("fs", "tp"),
        P("tp", "fs"),
        P("fs", "tp"),
    )
    out_specs = (P("fs", None), P("fs", "tp"), P("fs", "tp"), P("tp", "fs"), P("fs", "tp"))
    square_chips = mesh.shape["tp"] == 2 and mesh.shape["fs"] % 4 == 0 and mesh.shape["fs"] >= 8
    chosen = fused_body if square_chips else body
    return jax.shard_map(chosen, mesh=mesh, in_specs=in_specs, out_specs=out_specs, check_vma=False)
```

profile of v0, /device:TPU:0, one launch (start us, length us, event | category | flops | bytes accessed | tf_op | source)
XLA Modules:
  0.0 105.6 jit_solution(10523230525857273821)
XLA Ops:
  0.6 0.0 copy-start
  0.6 98.0 %shard_map.119 = (bf16[128,4096]{1,0:T(8,128)(2,1)}, bf16[128,1024]{1,0:T(8,128)(2,1)}, bf16[128,1024]{1,0:T(8,128)(2,1)}, f32[1024,256]{1,0:T(8,128)}, f32[256,1024]{1,0:T(8,128)}) custom-call(bf16[128,1024]{1,0:T(8,128)(2,1)} %refs_0_.1, bf16[1024,256]{1,0:T(8,128)(2,1)} %refs_1_.1, bf16[256,1024]{1,0:T(8,128)(2,1)} %refs_2_.1, bf16[128,1024]{1,0:T(8,128)(2,1)} %refs_3_.1, ...), custom_call_target="tpu_custom_call" | custom-call | flops 6442450944 | bytes 16777216 | tf_op jit(solution)/shard_map/pallas_call | solution.py:396
  98.7 0.0 copy-done
  98.7 0.0 copy-start.1
  98.7 0.0 copy-start.2
  98.7 2.5 %add.6 = f32[1024,256]{1,0:T(8,128)} add(f32[1024,256]{1,0:T(8,128)S(1)} %copy-done, f32[1024,256]{1,0:T(8,128)} %get-tuple-element.13) | non-fusion elementwise | flops 262144 | bytes 3145728 | tf_op jit(solution)/shard_map/add | solution.py:412
  101.2 0.0 copy-done.1
  101.2 0.0 copy-done.2
  101.2 0.0 copy-start.3
  101.2 1.1 %add.7 = f32[256,1024]{1,0:T(8,128)} add(f32[256,1024]{1,0:T(8,128)S(1)} %copy-done.1, f32[256,1024]{1,0:T(8,128)S(1)} %copy-done.2) | non-fusion elementwise | flops 262144 | bytes 3145728 | tf_op jit(solution)/shard_map/add | solution.py:412
  102.3 0.5 copy-done.3
  102.8 0.0 copy-start.5
  102.8 1.0 copy.16
  103.8 0.1 copy-done.5
  103.9 0.0 copy-start.4
  103.9 0.7 copy.17
  104.6 0.3 copy-done.4
  104.9 0.7 copy.18
Async XLA Ops:
  0.6 98.0 %copy-start = (f32[1024,256]{1,0:T(8,128)S(1)}, f32[1024,256]{1,0:T(8,128)}, u32[]{:S(2)}) copy-start(f32[1024,256]{1,0:T(8,128)} %param.14) | copy-start | bytes 3145732
  98.7 2.5 %copy-start.1 = (f32[256,1024]{1,0:T(8,128)S(1)}, f32[256,1024]{1,0:T(8,128)}, u32[]{:S(2)}) copy-start(f32[256,1024]{1,0:T(8,128)} %param.15) | copy-start | bytes 3145732
  98.7 2.5 %copy-start.2 = (f32[256,1024]{1,0:T(8,128)S(1)}, f32[256,1024]{1,0:T(8,128)}, u32[]{:S(2)}) copy-start(f32[256,1024]{1,0:T(8,128)} %get-tuple-element.14) | copy-start | bytes 3145732
  101.2 1.6 %copy-start.3 = (bf16[128,4096]{1,0:T(8,128)(2,1)S(1)}, bf16[128,4096]{1,0:T(8,128)(2,1)}, u32[]{:S(2)}) copy-start(bf16[128,4096]{1,0:T(8,128)(2,1)} %get-tuple-element.20) | copy-start | bytes 3145732
  102.8 1.1 %copy-start.5 = (bf16[128,1024]{1,0:T(8,128)(2,1)S(1)}, bf16[128,1024]{1,0:T(8,128)(2,1)}, u32[]{:S(2)}) copy-start(bf16[128,1024]{1,0:T(8,128)(2,1)} %get-tuple-element.21) | copy-start | bytes 786436
  103.9 1.0 copy-start.4
where the time goes:
time: 106 us
  Pallas kernels  98 us (92%)
  other arithmetic  3.58 us (3%)
  local copies, waits for them, and re-layouts  3.35 us (3%)
    pallas_call x1, Pallas kernels, fused_body(): pl.pallas_call(lambda *refs: fused(a, *refs), out_shape=(jax.ShapeDtypeSt...  98 us
    unnamed x15, local copies, waits for them, and re-layouts  3.35 us
    add x1, other arithmetic, fused_body(): up_sum + up_grad  2.48 us

commit v1 on v0

v1 whole, which is shorter than its diff:
```python
import jax
import jax.numpy as jnp
from jax import lax
from jax.experimental import pallas as pl
from jax.experimental.pallas import tpu as pltpu
from jax.sharding import PartitionSpec as P

MESH = pl.DeviceIdType.MESH
F32 = jnp.float32
BF16 = jnp.bfloat16


def dot(left, right, lc, rc):
    return lax.dot_general(left, right, (((lc,), (rc,)), ((), ())), preferred_element_type=F32)


def square_relu(value):
    kept = jnp.maximum(value.astype(F32), 0.0)
    return (kept * kept).astype(BF16)


def fused(a, late_in, up_w, down_w, early_in, early_pre, cot,
          late_pre_o, late_out_o, in_grad_o, up_o, down_o,
          cot_g, late_g, early_g, pre_g, up_g, down_g, gt_s, gt_r, pg, eh, lt_s, lt_r, lp, lh, lp_g,
          part, ig_s, ig_u, ig_d, lo_s, lo_u, lo_d,
          dg_s, dg_x, dg_y, dg_fx, dg_fy, ug_s, ug_x, ug_y, ug_fx, ug_fy,
          ag_ss, ag_rs, w_ss, w_rs, e_ss, e_rs, l_ss, l_rs, t_ss, t_rs, rl_ss, rl_rs, rq_ss, rq_rs,
          local_s, down_v, up_v, ig_v, lo_v):
    side = 4
    half_side = side // 2
    me = lax.axis_index("fs")
    t = lax.axis_index("tp")
    z = me // side
    q = lax.rem(me, side)
    y = q // 2
    x = lax.rem(q, 2)
    qx = y * 2 + (1 - x)
    qy = (1 - y) * 2 + x
    qd = side - 1 - q
    xn = (z * side + qx, t)
    yn = (z * side + qy, t)
    pn = (me, 1 - t)
    above = (lax.rem(me + side, a * side), t)
    below = (lax.rem(me + (a - 1) * side, a * side), t)
    rows = late_in.shape[0]
    ff = up_w.shape[1]
    width = late_in.shape[1]
    cut = width // 2
    last = a - 1
    middle = (z > 0) & (z < last)

    def begin(src, dst, k):
        copy = pltpu.make_async_copy(src, dst, local_s.at[k])
        copy.start()
        return copy

    def slot(j):
        return pl.ds(pl.multiple_of(j * rows, rows), rows)

    def slots(n):
        size = rows // n
        return lambda j, c: pl.ds(pl.multiple_of(j * rows + c * size, size), size)

    def columns(block, unit):
        return pl.ds(pl.multiple_of(block * unit, unit), unit)

    own_rows = slot(z)
    own_down = begin(down_w, down_g.at[q], 0)
    own_cot = begin(cot, cot_g.at[own_rows], 1)
    own_late = begin(late_in, late_g.at[own_rows], 3)
    own_early = [begin(early_in.at[:, pl.ds(c * cut, cut)], early_g.at[c, own_rows], 14 + c) for c in range(2)]
    own_up = begin(up_w, up_g.at[q], 2)
    own_pre = [
        begin(early_pre.at[:, pl.ds(pl.multiple_of((z * side + b) * ff, ff), ff)],
              pre_g.at[b, own_rows], 5 + b)
        for b in range(side)
    ]

    barrier = pltpu.get_barrier_semaphore()
    greet = [xn, yn, pn] + [(lax.rem(me + o * side, a * side), t) for o in range(1, a)]
    for device in greet:
        pl.semaphore_signal(barrier, inc=1, device_id=device, device_id_type=MESH)
    pl.semaphore_wait(barrier, len(greet))

    sent = []

    def run(cond, go):
        if cond is None:
            go()
        else:
            pl.when(cond)(go)

    def rc(src, dst, ss, rs, device):
        return pltpu.make_async_remote_copy(
            src_ref=src, dst_ref=dst, send_sem=ss, recv_sem=rs, device_id=device, device_id_type=MESH)

    def send(src, dst, ss, rs, device, cond=None):
        copy = rc(src, dst, ss, rs, device)
        run(cond, copy.start)
        sent.append((cond, copy))

    def arrive(dst, ss, rs, cond=None):
        run(cond, rc(dst, dst, ss, rs, pn).wait_recv)

    gathers = {
        "cot": (0, 2, lambda j, c: cot_g.at[slots(2)(j, c)]),
        "late": (2, 2, lambda j, c: late_g.at[slots(2)(j, c)]),
        "early0": (4, 1, lambda j, c: early_g.at[0, slot(j)]),
        "early1": (5, 1, lambda j, c: early_g.at[1, slot(j)]),
    }

    def gather_own(name, depth=None):
        first, pieces, piece = gathers[name]
        for c in range(pieces):
            own = piece(z, c)
            for way, edge, device in ((0, z < last, above), (1, z > 0, below)):
                left = z if way == 0 else last - z
                cond = edge if depth is None else edge & (left == depth)
                send(own, own, ag_ss.at[first + c, way, 0], ag_rs.at[first + c, way, 1], device, cond)

    def gather_relay(name, d, some=None):
        if d >= last:
            return
        first, pieces, piece = gathers[name]
        for c in range(pieces) if some is None else some:
            for way, here, j, device in ((0, (z >= d) & (z < last), z - d, above),
                                         (1, (z + d < a) & (z > 0), z + d, below)):
                place = piece(jnp.clip(j, 0, last), c)
                arrive(place, ag_ss.at[first + c, way, 0], ag_rs.at[first + c, way, d], here)
                send(place, place, ag_ss.at[first + c, way, d], ag_rs.at[first + c, way, d + 1], device, here)

    def gather_end(name):
        first, pieces, piece = gathers[name]
        for d in range(1, a):
            for c in range(pieces):
                for way, here, j in ((0, z == last, z - d), (1, z == 0, z + d)):
                    place = piece(jnp.clip(j, 0, last), c)
                    arrive(place, ag_ss.at[first + c, way, 0], ag_rs.at[first + c, way, d], here)

    def half(ref, block, h):
        n = ref.shape[1] // 2
        return ref.at[block, pl.ds(h * n, n)]

    def half2(ref, h):
        n = ref.shape[0] // 2
        return ref.at[pl.ds(h * n, n)]

    def square_send(which, own, buf):
        for h in (0, 1):
            send(half2(own, h), half(buf, q, h), w_ss.at[which, 0, h], w_rs.at[which, 0, h], xn)
            send(half2(own, 1 - h), half(buf, q, 1 - h), w_ss.at[which, 1, 1 - h], w_rs.at[which, 1, 1 - h], yn)

    def square_relay(which, buf):
        arrive(half(buf, qx, 0), w_ss.at[which, 0, 0], w_rs.at[which, 0, 0])
        send(half(buf, qx, 0), half(buf, qx, 0), w_ss.at[which, 1, 2], w_rs.at[which, 1, 2], yn)
        arrive(half(buf, qy, 1), w_ss.at[which, 0, 0], w_rs.at[which, 1, 1])
        send(half(buf, qy, 1), half(buf, qy, 1), w_ss.at[which, 0, 2], w_rs.at[which, 0, 2], xn)

    def square_rest(which, buf):
        arrive(half(buf, qx, 1), w_ss.at[which, 0, 0], w_rs.at[which, 0, 1])
        arrive(half(buf, qy, 0), w_ss.at[which, 0, 0], w_rs.at[which, 1, 0])
        arrive(half(buf, qd, 0), w_ss.at[which, 0, 0], w_rs.at[which, 1, 2])
        arrive(half(buf, qd, 1), w_ss.at[which, 0, 0], w_rs.at[which, 0, 2])

    def square_sum(which, c, block, staged, first_x, first_y, fin_x, fin_y, out):
        n = staged.shape[1] // 2
        sems = lambda k: (rq_ss.at[which, c, k], rq_rs.at[which, c, k])
        wait = lambda dst, k: arrive(dst, *sems(k))

        def start():
            staged[qd] = block(qd).astype(BF16)
            send(half(staged, qd, 0), first_x, *sems(0), xn)
            send(half(staged, qd, 1), first_y, *sems(1), yn)
            staged[qx] = block(qx).astype(BF16)
            send(half(staged, qx, 0), half2(fin_x, 0), *sems(2), xn)
            staged[qy] = block(qy).astype(BF16)
            send(half(staged, qy, 1), half2(fin_y, 1), *sems(3), yn)

        def relay():
            wait(first_x, 0)
            staged[qy, 0:n] = (staged[qy, 0:n].astype(F32) + first_x[...].astype(F32)).astype(BF16)
            send(half(staged, qy, 0), half2(fin_y, 0), *sems(4), yn)
            wait(first_y, 1)
            staged[qx, n:2 * n] = (staged[qx, n:2 * n].astype(F32) + first_y[...].astype(F32)).astype(BF16)
            send(half(staged, qx, 1), half2(fin_x, 1), *sems(5), xn)

        def own():
            out[...] = block(q)

        def finish():
            wait(half2(fin_x, 0), 2)
            wait(half2(fin_y, 1), 3)
            wait(half2(fin_y, 0), 4)
            wait(half2(fin_x, 1), 5)
            out[...] = out[...] + (fin_x[...].astype(F32) + fin_y[...].astype(F32))

        return start, relay, own, finish

    def line_sum(which, c, value, staged, from_u, from_d, out):
        own = part.at[which, c]

        def go(way, j, step, cond):
            buf, device = ((from_u, above), (from_d, below))[way]
            send(staged.at[c, j], buf.at[c, j], rl_ss.at[which, c, way, step], rl_rs.at[which, c, way, j], device, cond)

        def start():
            own[...] = value(c)
            for j in range(a):
                staged[c, j] = own[pl.ds(j * rows, rows)].astype(BF16)
            for step in range(last):
                go(0, last - step, step, z == 0)
                go(1, step, step, z == last)

        def relay(step, opening):
            if step >= last:
                return
            for way in range(2):
                if way == 0:
                    j, on, opens, buf = last + z - step, step >= z, z == step, from_u
                else:
                    j, on, opens, buf = step - (last - z), step >= last - z, last - z == step, from_d
                on = on & middle & (opens if opening else jnp.logical_not(opens))
                j = jnp.clip(j, 0, last)

                @pl.when(on)
                def _(j=j, buf=buf, way=way):
                    arrive(buf.at[c, j], rl_ss.at[which, 0, 0, 0], rl_rs.at[which, c, way, j])
                    staged[c, j] = (staged[c, j].astype(F32) + buf[c, j].astype(F32)).astype(BF16)

                go(way, j, step, on)

        def finish():
            @pl.when(z > 0)
            def _():
                arrive(from_u.at[c, z], rl_ss.at[which, 0, 0, 0], rl_rs.at[which, c, 0, z])
                own[own_rows] = own[own_rows] + from_u[c, z].astype(F32)

            @pl.when(z < last)
            def _():
                arrive(from_d.at[c, z], rl_ss.at[which, 0, 0, 0], rl_rs.at[which, c, 1, z])
                own[own_rows] = own[own_rows] + from_d[c, z].astype(F32)

            out[:, pl.ds(c * cut, cut)] = own[own_rows].astype(BF16)

        return start, relay, finish

    def hops(b_of, go, offsets=None):
        for o in range(1, a) if offsets is None else offsets:
            if o < a:
                zs = lax.rem(z - o + a, a)
                for u in range(half_side):
                    go(o, u, zs, b_of(u))

    mine = lambda u: t * half_side + u
    other = lambda u: (1 - t) * half_side + u

    def pre_relay(o, u, zs, b):
        place = pre_g.at[b, slot(zs)]
        arrive(place, e_ss.at[0, 0, 0], e_rs.at[0, o, u])
        send(place, place, e_ss.at[1, o, u], e_rs.at[1, o, u], pn)

    def pre_rest(o, u, zs, b):
        arrive(pre_g.at[b, slot(zs)], e_ss.at[0, 0, 0], e_rs.at[1, o, u])

    def out_relay(o, u, zs, b):
        place = lp_g.at[:, columns(zs * side + b, ff)]
        arrive(place, l_ss.at[0, 0, 0], l_rs.at[0, o, u])
        send(place, place, l_ss.at[1, o, u], l_rs.at[1, o, u], pn)

    def out_rest(o, u, zs, b):
        arrive(lp_g.at[:, columns(zs * side + b, ff)], l_ss.at[0, 0, 0], l_rs.at[1, o, u])

    def ig_value(c):
        return sum(dot(pg[b], up_g[b, pl.ds(c * cut, cut), :], 1, 1) for b in range(side))

    def lo_value(c):
        return sum(dot(lh[b], down_g[b, :, pl.ds(c * cut, cut)], 1, 0) for b in range(side))

    ig = [line_sum(0, c, ig_value, ig_s, ig_u, ig_d, ig_v) for c in range(2)]
    lo = [line_sum(1, c, lo_value, lo_s, lo_u, lo_d, lo_v) for c in range(2)]
    dg = square_sum(1, 0, lambda b: dot(eh[b], cot_g[...], 0, 0), dg_s, dg_x, dg_y, dg_fx, dg_fy, down_v)
    ug = [
        square_sum(0, c, lambda b, c=c: dot(early_g[c], pg[b], 0, 0), ug_s.at[c], ug_x.at[c], ug_y.at[c],
                   ug_fx.at[c], ug_fy.at[c], up_v.at[pl.ds(c * cut, cut)])
        for c in range(2)
    ]

    own_down.wait()
    square_send(1, down_g.at[q], down_g)
    own_cot.wait()
    gather_own("cot")
    for o in range(1, a):
        zd = lax.rem(z + o, a)
        for u in range(half_side):
            b = mine(u)
            send(early_pre.at[:, columns(zd * side + b, ff)], pre_g.at[b, slot(z)],
                 e_ss.at[0, o, u], e_rs.at[0, o, u], (zd * side + q, t))
    own_late.wait()
    gather_own("late", 0)
    for copy in own_early:
        copy.wait()
    gather_own("early0", 0)
    gather_own("early1", 0)
    own_up.wait()
    for copy in own_pre:
        copy.wait()
    gather_relay("cot", 1)
    gather_own("late", 1)
    square_relay(1, down_g)
    square_send(0, up_g.at[q], up_g)
    for d in range(2, last):
        gather_relay("cot", d)
        gather_own("late", d)
    hops(mine, pre_relay, (1,))
    gather_relay("late", 1, (0,))
    gather_end("cot")
    square_rest(1, down_g)

    @pl.loop(0, side)
    def _(b):
        gt_s[b] = dot(cot_g[...], down_g[b], 1, 1).astype(BF16)

    send(gt_s, gt_r, t_ss.at[0], t_rs.at[0], pn)
    square_relay(0, up_g)
    hops(mine, pre_relay, range(2, a))
    gather_relay("late", 1, (1,))
    gather_own("early0", 1)
    gather_own("early1", 1)
    hops(other, pre_rest)

    @pl.loop(0, side)
    def _(b):
        eh[b] = square_relu(pre_g[b])

    arrive(gt_r, t_ss.at[0], t_rs.at[0])

    @pl.loop(0, side)
    def _(b):
        hidden = gt_s[b].astype(F32) + gt_r[b].astype(F32)
        pg[b] = (hidden * 2.0 * jnp.maximum(pre_g[b].astype(F32), 0.0)).astype(BF16)

    dg_start, dg_relay, dg_own, dg_finish = dg
    dg_start()
    gather_relay("early0", 1)
    square_rest(0, up_g)
    ig[0][0]()
    gather_relay("late", 2, (0,))
    ig[1][0]()
    dg_relay()
    gather_relay("late", 2, (1,))
    for d in range(3, last):
        gather_relay("late", d)
    for d in range(2, last):
        gather_own("early0", d)
        gather_own("early1", d)
    gather_relay("early1", 1)
    ig[0][1](1, True)
    gather_end("late")

    @pl.loop(0, side)
    def _(b):
        lt_s[b] = dot(late_g[...], up_g[b], 1, 0).astype(BF16)

    send(lt_s, lt_r, t_ss.at[1], t_rs.at[1], pn)
    ig[0][1](2, False)
    for d in range(2, last):
        gather_relay("early0", d)
    arrive(lt_r, t_ss.at[1], t_rs.at[1])

    @pl.loop(0, side)
    def _(b):
        pre = (lt_s[b].astype(F32) + lt_r[b].astype(F32)).astype(BF16)
        lp[b] = pre
        lh[b] = square_relu(pre)

    lo[0][0]()
    lo[1][0]()
    for o in range(1, a):
        zd = lax.rem(z + o, a)
        for u in range(half_side):
            b = mine(u)
            send(lp.at[b, slot(zd)], lp_g.at[:, columns(z * side + b, ff)],
                 l_ss.at[0, o, u], l_rs.at[0, o, u], (zd * side + q, t))
    ig[1][1](1, True)
    for d in range(2, last):
        gather_relay("early1", d)
    gather_end("early0")
    ug[0][0]()
    ig[1][1](2, False)
    ig[0][1](2, True)
    lo[0][1](1, True)
    dg_own()
    dg_finish()
    out_down = begin(down_v, down_o, 9)
    ug[0][1]()
    ig[1][1](2, True)
    for k in range(3, last):
        for c in range(2):
            for opening in (False, True):
                ig[c][1](k, opening)
    gather_end("early1")
    ug[1][0]()
    lo[0][1](2, False)
    lo[0][1](2, True)
    lo[1][1](1, True)
    ug[1][1]()
    ig[0][2]()
    ig[1][2]()
    out_ig = begin(ig_v, in_grad_o, 10)
    lo[1][1](2, False)
    lo[1][1](2, True)
    for k in range(3, last):
        for c in range(2):
            for opening in (False, True):
                lo[c][1](k, opening)
    for b in range(side):
        lp_g[:, columns(z * side + b, ff)] = lp[b, slot(z)]
    ug[0][2]()
    ug[1][2]()
    hops(mine, out_relay)
    ug[0][3]()
    lo[0][2]()
    ug[1][3]()
    out_up = begin(up_v, up_o, 13)
    lo[1][2]()
    out_lo = begin(lo_v, late_out_o, 12)
    hops(other, out_rest)
    out_pre = begin(lp_g, late_pre_o, 11)

    for cond, copy in sent:
        run(cond, copy.wait_send)
    for copy in (out_down, out_ig, out_pre, out_lo, out_up):
        copy.wait()


def fused_body(late_input, up_weight, down_weight, early_input, early_pre, cotangent, up_sum, down_sum):
    a = lax.axis_size("fs") // 4
    side = 4
    rows, width = late_input.shape
    ff = up_weight.shape[1]
    tokens, hidden = rows * a, ff * side
    cut = width // 2
    V = pltpu.VMEM
    D = pltpu.SemaphoreType.DMA
    token_block = V((tokens, width), BF16)
    hidden_block = V((side, tokens, ff), BF16)
    line_block = V((2, a, rows, cut), BF16)
    scratch = (
        [token_block] * 2
        + [V((2, tokens, cut), BF16)]
        + [hidden_block, V((side, width, ff), BF16), V((side, ff, width), BF16)]
        + [hidden_block] * 8
        + [V((rows, hidden * a), BF16), V((2, 2, tokens, cut), F32)]
        + [line_block] * 6
        + [V((side, ff, width), BF16)] + [V((ff // 2, width), BF16)] * 2 + [V((ff, width), BF16)] * 2
        + [V((2, side, cut, ff), BF16)] + [V((2, cut // 2, ff), BF16)] * 2 + [V((2, cut, ff), BF16)] * 2
        + [D((6, 2, a)), D((6, 2, a)), D((2, 2, 3)), D((2, 2, 3)), D((2, a, 2)), D((2, a, 2)),
           D((2, a, 2)), D((2, a, 2)), D((2,)), D((2,)), D((2, 2, 2, a)), D((2, 2, 2, a)),
           D((2, 2, 6)), D((2, 2, 6)), D((16,))]
        + [V((ff, width), F32), V((width, ff), F32)] + [V((rows, width), BF16)] * 2
    )
    flops = 12 * tokens * hidden * width
    late_pre, late_out, input_grad, up_grad, down_grad = pl.pallas_call(
        lambda *refs: fused(a, *refs),
        out_shape=(
            jax.ShapeDtypeStruct(early_pre.shape, BF16),
            jax.ShapeDtypeStruct(late_input.shape, BF16),
            jax.ShapeDtypeStruct(early_input.shape, BF16),
            jax.ShapeDtypeStruct(up_sum.shape, F32),
            jax.ShapeDtypeStruct(down_sum.shape, F32),
        ),
        in_specs=[pl.BlockSpec(memory_space=pl.ANY)] * 6,
        out_specs=[pl.BlockSpec(memory_space=pl.ANY)] * 5,
        scratch_shapes=scratch,
        compiler_params=pltpu.CompilerParams(
            collective_id=0, has_side_effects=True, vmem_limit_bytes=62 * 1024 * 1024),
        cost_estimate=pl.CostEstimate(flops=flops, bytes_accessed=1 << 24, transcendentals=0),
    )(late_input, up_weight, down_weight, early_input, early_pre, cotangent)
    return late_pre, late_out, input_grad, up_sum + up_grad, down_sum + down_grad


def contract_rows(left, right):
    return lax.dot_general(
        left, right, (((0,), (0,)), ((), ())), preferred_element_type=jnp.float32
    )


def contract_cols(left, right):
    return lax.dot_general(
        left, right, (((1,), (1,)), ((), ())), preferred_element_type=jnp.float32
    )


def body(late_input, up_weight, down_weight, early_input, early_pre, cotangent, up_sum, down_sum):
    up_gathered = lax.all_gather(up_weight, "fs", axis=1, tiled=True)
    down_gathered = lax.all_gather(down_weight, "fs", axis=0, tiled=True)
    pre_terms = jnp.dot(late_input, up_gathered, preferred_element_type=jnp.float32)
    pre_summed = lax.psum(pre_terms.astype(jnp.bfloat16), "tp")
    late_hidden = jnp.square(jax.nn.relu(pre_summed.astype(jnp.float32))).astype(jnp.bfloat16)
    early_float = early_pre.astype(jnp.float32)
    early_hidden = jnp.square(jax.nn.relu(early_float)).astype(jnp.bfloat16)
    late_out = jnp.dot(late_hidden, down_gathered, preferred_element_type=jnp.float32).astype(
        jnp.bfloat16
    )
    grad_terms = contract_cols(cotangent, down_gathered)
    hidden_grad = lax.psum(grad_terms.astype(jnp.bfloat16), "tp").astype(jnp.float32)
    pre_grad = (hidden_grad * 2.0 * jax.nn.relu(early_float)).astype(jnp.bfloat16)
    input_grad = contract_cols(pre_grad, up_gathered).astype(jnp.bfloat16)
    grad_local, hidden_local = (
        lax.all_to_all(pre_grad, "fs", split_axis=1, concat_axis=0, tiled=True),
        lax.all_to_all(early_hidden, "fs", split_axis=1, concat_axis=0, tiled=True),
    )
    rows = grad_local
    up_grad = contract_rows(lax.all_gather(early_input, "fs", axis=0, tiled=True), rows)
    up_total = up_sum + up_grad
    rows = hidden_local
    down_grad = contract_rows(rows, lax.all_gather(cotangent, "fs", axis=0, tiled=True))
    down_total = down_sum + down_grad
    return (pre_summed, late_out, input_grad, up_total, down_total)


def solution(mesh):
    in_specs = (
        P("fs", "tp"),
        P("tp", "fs"),
        P("fs", "tp"),
        P("fs", "tp"),
        P("fs", None),
        P("fs", "tp"),
        P("tp", "fs"),
        P("fs", "tp"),
    )
    out_specs = (P("fs", None), P("fs", "tp"), P("fs", "tp"), P("tp", "fs"), P("fs", "tp"))
    square_chips = mesh.shape["tp"] == 2 and mesh.shape["fs"] % 4 == 0 and mesh.shape["fs"] >= 8
    chosen = fused_body if square_chips else body
    return jax.shard_map(chosen, mesh=mesh, in_specs=in_specs, out_specs=out_specs, check_vma=False)
```

time: 106 us -> 99 us (0.934)
  Pallas kernels: 98 us -> 91.2 us
    pallas_call x1, Pallas kernels: 98 us -> 91.2 us  [fused_body(): pl.pallas_call(lambda *refs: fused(a, *refs), out_shape=(jax.ShapeDtypeSt...]
where the time goes in v1:
time: 99 us; the launch traced here: 98.8 us
  Pallas kernels  91.2 us (92%)
  other arithmetic  3.58 us (4%)
  local copies, waits for them, and re-layouts  3.35 us (3%)
    pallas_call x1, Pallas kernels, fused_body(): pl.pallas_call(lambda *refs: fused(a, *refs), out_shape=(jax.ShapeDtypeSt...  91.2 us
    unnamed x15, local copies, waits for them, and re-layouts  3.35 us
    add x1, other arithmetic, fused_body(): up_sum + up_grad  2.48 us

profile of v1, /device:TPU:0, one launch (start us, length us, event | category | flops | bytes accessed | tf_op | source)
XLA Modules:
  0.0 98.8 jit_solution(18388627491635651431)
XLA Ops:
  0.6 0.0 copy-start
  0.6 91.2 %shard_map.119 = (bf16[128,4096]{1,0:T(8,128)(2,1)}, bf16[128,1024]{1,0:T(8,128)(2,1)}, bf16[128,1024]{1,0:T(8,128)(2,1)}, f32[1024,256]{1,0:T(8,128)}, f32[256,1024]{1,0:T(8,128)}) custom-call(bf16[128,1024]{1,0:T(8,128)(2,1)} %refs_0_.1, bf16[1024,256]{1,0:T(8,128)(2,1)} %refs_1_.1, bf16[256,1024]{1,0:T(8,128)(2,1)} %refs_2_.1, bf16[128,1024]{1,0:T(8,128)(2,1)} %refs_3_.1, ...), custom_call_target="tpu_custom_call" | custom-call | flops 6442450944 | bytes 16777216 | tf_op jit(solution)/shard_map/pallas_call | solution.py:463
  91.8 0.0 copy-done
  91.9 0.0 copy-start.1
  91.9 0.0 copy-start.2
  91.9 2.5 %add.6 = f32[1024,256]{1,0:T(8,128)} add(f32[1024,256]{1,0:T(8,128)S(1)} %copy-done, f32[1024,256]{1,0:T(8,128)} %get-tuple-element.13) | non-fusion elementwise | flops 262144 | bytes 3145728 | tf_op jit(solution)/shard_map/add | solution.py:479
  94.4 0.0 copy-done.1
  94.4 0.0 copy-done.2
  94.4 0.0 copy-start.3
  94.4 1.1 %add.7 = f32[256,1024]{1,0:T(8,128)} add(f32[256,1024]{1,0:T(8,128)S(1)} %copy-done.1, f32[256,1024]{1,0:T(8,128)S(1)} %copy-done.2) | non-fusion elementwise | flops 262144 | bytes 3145728 | tf_op jit(solution)/shard_map/add | solution.py:479
  95.5 0.5 copy-done.3
  96.0 0.0 copy-start.5
  96.0 1.0 copy.16
  96.9 0.1 copy-done.5
  97.1 0.0 copy-start.4
  97.1 0.7 copy.17
  97.8 0.3 copy-done.4
  98.1 0.7 copy.18
Async XLA Ops:
  0.6 91.2 %copy-start = (f32[1024,256]{1,0:T(8,128)S(1)}, f32[1024,256]{1,0:T(8,128)}, u32[]{:S(2)}) copy-start(f32[1024,256]{1,0:T(8,128)} %param.14) | copy-start | bytes 3145732
  91.9 2.5 %copy-start.1 = (f32[256,1024]{1,0:T(8,128)S(1)}, f32[256,1024]{1,0:T(8,128)}, u32[]{:S(2)}) copy-start(f32[256,1024]{1,0:T(8,128)} %param.15) | copy-start | bytes 3145732
  91.9 2.5 %copy-start.2 = (f32[256,1024]{1,0:T(8,128)S(1)}, f32[256,1024]{1,0:T(8,128)}, u32[]{:S(2)}) copy-start(f32[256,1024]{1,0:T(8,128)} %get-tuple-element.14) | copy-start | bytes 3145732
  94.4 1.6 %copy-start.3 = (bf16[128,4096]{1,0:T(8,128)(2,1)S(1)}, bf16[128,4096]{1,0:T(8,128)(2,1)}, u32[]{:S(2)}) copy-start(bf16[128,4096]{1,0:T(8,128)(2,1)} %get-tuple-element.20) | copy-start | bytes 3145732
  96.0 1.1 %copy-start.5 = (bf16[128,1024]{1,0:T(8,128)(2,1)S(1)}, bf16[128,1024]{1,0:T(8,128)(2,1)}, u32[]{:S(2)}) copy-start(bf16[128,1024]{1,0:T(8,128)(2,1)} %get-tuple-element.21) | copy-start | bytes 786436
  97.1 1.0 %copy-start.4 = (bf16[128,1024]{1,0:T(8,128)(2,1)S(1)}, bf16[128,1024]{1,0:T(8,128)(2,1)}, u32[]{:S(2)}) copy-start(bf16[128,1024]{1,0:T(8,128)(2,1)} %get-tuple-element.22) | copy-start | bytes 786436

commit v2 on v1

--- a/solution.py
+++ b/solution.py
@@ -19,13 +19,13 @@
     return (kept * kept).astype(BF16)
 
 
-def fused(a, late_in, up_w, down_w, early_in, early_pre, cot,
-          late_pre_o, late_out_o, in_grad_o, up_o, down_o,
+def fused(a, late_in, up_w, down_w, early_in, early_pre, cot, up_old, down_old,
+          late_pre_o, lo_v, ig_v, up_v, down_v,
           cot_g, late_g, early_g, pre_g, up_g, down_g, gt_s, gt_r, pg, eh, lt_s, lt_r, lp, lh, lp_g,
           part, ig_s, ig_u, ig_d, lo_s, lo_u, lo_d,
           dg_s, dg_x, dg_y, dg_fx, dg_fy, ug_s, ug_x, ug_y, ug_fx, ug_fy,
           ag_ss, ag_rs, w_ss, w_rs, e_ss, e_rs, l_ss, l_rs, t_ss, t_rs, rl_ss, rl_rs, rq_ss, rq_rs,
-          local_s, down_v, up_v, ig_v, lo_v):
+          local_s, up_was, down_was):
     side = 4
     half_side = side // 2
     me = lax.axis_index("fs")
@@ -68,13 +68,15 @@
     own_down = begin(down_w, down_g.at[q], 0)
     own_cot = begin(cot, cot_g.at[own_rows], 1)
     own_late = begin(late_in, late_g.at[own_rows], 3)
-    own_early = [begin(early_in.at[:, pl.ds(c * cut, cut)], early_g.at[c, own_rows], 14 + c) for c in range(2)]
+    own_early = [begin(early_in.at[:, pl.ds(c * cut, cut)], early_g.at[c, own_rows], 9 + c) for c in range(2)]
     own_up = begin(up_w, up_g.at[q], 2)
     own_pre = [
         begin(early_pre.at[:, pl.ds(pl.multiple_of((z * side + b) * ff, ff), ff)],
               pre_g.at[b, own_rows], 5 + b)
         for b in range(side)
     ]
+
+    own_sums = [begin(up_old, up_was, 11), begin(down_old, down_was, 12)]
 
     barrier = pltpu.get_barrier_semaphore()
     greet = [xn, yn, pn] + [(lax.rem(me + o * side, a * side), t) for o in range(1, a)]
@@ -162,7 +164,7 @@
         arrive(half(buf, qd, 0), w_ss.at[which, 0, 0], w_rs.at[which, 1, 2])
         arrive(half(buf, qd, 1), w_ss.at[which, 0, 0], w_rs.at[which, 0, 2])
 
-    def square_sum(which, c, block, staged, first_x, first_y, fin_x, fin_y, out):
+    def square_sum(which, c, block, staged, first_x, first_y, fin_x, fin_y, was, out):
         n = staged.shape[1] // 2
         sems = lambda k: (rq_ss.at[which, c, k], rq_rs.at[which, c, k])
         wait = lambda dst, k: arrive(dst, *sems(k))
@@ -192,7 +194,7 @@
             wait(half2(fin_y, 1), 3)
             wait(half2(fin_y, 0), 4)
             wait(half2(fin_x, 1), 5)
-            out[...] = out[...] + (fin_x[...].astype(F32) + fin_y[...].astype(F32))
+            out[...] = was[...] + (out[...] + (fin_x[...].astype(F32) + fin_y[...].astype(F32)))
 
         return start, relay, own, finish
 
@@ -278,10 +280,10 @@
 
     ig = [line_sum(0, c, ig_value, ig_s, ig_u, ig_d, ig_v) for c in range(2)]
     lo = [line_sum(1, c, lo_value, lo_s, lo_u, lo_d, lo_v) for c in range(2)]
-    dg = square_sum(1, 0, lambda b: dot(eh[b], cot_g[...], 0, 0), dg_s, dg_x, dg_y, dg_fx, dg_fy, down_v)
+    dg = square_sum(1, 0, lambda b: dot(eh[b], cot_g[...], 0, 0), dg_s, dg_x, dg_y, dg_fx, dg_fy, down_was, down_v)
     ug = [
         square_sum(0, c, lambda b, c=c: dot(early_g[c], pg[b], 0, 0), ug_s.at[c], ug_x.at[c], ug_y.at[c],
-                   ug_fx.at[c], ug_fy.at[c], up_v.at[pl.ds(c * cut, cut)])
+                   ug_fx.at[c], ug_fy.at[c], up_was.at[pl.ds(c * cut, cut)], up_v.at[pl.ds(c * cut, cut)])
         for c in range(2)
     ]
 
@@ -390,8 +392,9 @@
     ig[0][1](2, True)
     lo[0][1](1, True)
     dg_own()
+    for copy in own_sums:
+        copy.wait()
     dg_finish()
-    out_down = begin(down_v, down_o, 9)
     ug[0][1]()
     ig[1][1](2, True)
     for k in range(3, last):
@@ -406,7 +409,6 @@
     ug[1][1]()
     ig[0][2]()
     ig[1][2]()
-    out_ig = begin(ig_v, in_grad_o, 10)
     lo[1][1](2, False)
     lo[1][1](2, True)
     for k in range(3, last):
@@ -421,16 +423,34 @@
     ug[0][3]()
     lo[0][2]()
     ug[1][3]()
-    out_up = begin(up_v, up_o, 13)
     lo[1][2]()
-    out_lo = begin(lo_v, late_out_o, 12)
     hops(other, out_rest)
-    out_pre = begin(lp_g, late_pre_o, 11)
+    late_pre_o[...] = lp_g[...]
 
     for cond, copy in sent:
         run(cond, copy.wait_send)
-    for copy in (out_down, out_ig, out_pre, out_lo, out_up):
+
+
+def store_body(*refs):
+    n = len(refs) // 2
+    sems = refs[2 * n]
+    copies = [pltpu.make_async_copy(refs[k], refs[n + k], sems.at[k]) for k in range(n)]
+    for copy in copies:
+        copy.start()
+    for copy in copies:
         copy.wait()
+
+
+def store(results):
+    n = len(results)
+    return pl.pallas_call(
+        store_body,
+        out_shape=tuple(jax.ShapeDtypeStruct(r.shape, r.dtype) for r in results),
+        in_specs=[pl.BlockSpec(memory_space=pltpu.VMEM)] * n,
+        out_specs=[pl.BlockSpec(memory_space=pltpu.HBM)] * n,
+        scratch_shapes=[pltpu.SemaphoreType.DMA((n,))],
+        compiler_params=pltpu.CompilerParams(vmem_limit_bytes=16 * 1024 * 1024),
+    )(*results)
 
 
 def fused_body(late_input, up_weight, down_weight, early_input, early_pre, cotangent, up_sum, down_sum):
@@ -456,11 +476,11 @@
         + [V((2, side, cut, ff), BF16)] + [V((2, cut // 2, ff), BF16)] * 2 + [V((2, cut, ff), BF16)] * 2
         + [D((6, 2, a)), D((6, 2, a)), D((2, 2, 3)), D((2, 2, 3)), D((2, a, 2)), D((2, a, 2)),
            D((2, a, 2)), D((2, a, 2)), D((2,)), D((2,)), D((2, 2, 2, a)), D((2, 2, 2, a)),
-           D((2, 2, 6)), D((2, 2, 6)), D((16,))]
-        + [V((ff, width), F32), V((width, ff), F32)] + [V((rows, width), BF16)] * 2
+           D((2, 2, 6)), D((2, 2, 6)), D((13,))]
+        + [V((width, ff), F32), V((ff, width), F32)]
     )
     flops = 12 * tokens * hidden * width
-    late_pre, late_out, input_grad, up_grad, down_grad = pl.pallas_call(
+    results = pl.pallas_call(
         lambda *refs: fused(a, *refs),
         out_shape=(
             jax.ShapeDtypeStruct(early_pre.shape, BF16),
@@ -469,14 +489,15 @@
             jax.ShapeDtypeStruct(up_sum.shape, F32),
             jax.ShapeDtypeStruct(down_sum.shape, F32),
         ),
-        in_specs=[pl.BlockSpec(memory_space=pl.ANY)] * 6,
-        out_specs=[pl.BlockSpec(memory_space=pl.ANY)] * 5,
+        in_specs=[pl.BlockSpec(memory_space=pltpu.HBM)] * 8,
+        out_specs=[pl.BlockSpec(memory_space=pltpu.VMEM)] * 5,
         scratch_shapes=scratch,
         compiler_params=pltpu.CompilerParams(
-            collective_id=0, has_side_effects=True, vmem_limit_bytes=62 * 1024 * 1024),
+            collective_id=0, has_side_effects=True, vmem_limit_bytes=48 * 1024 * 1024),
         cost_estimate=pl.CostEstimate(flops=flops, bytes_accessed=1 << 24, transcendentals=0),
-    )(late_input, up_weight, down_weight, early_input, early_pre, cotangent)
-    return late_pre, late_out, input_grad, up_sum + up_grad, down_sum + down_grad
+    )(*[pltpu.with_memory_space_constraint(v, pltpu.HBM) for v in (
+        late_input, up_weight, down_weight, early_input, early_pre, cotangent, up_sum, down_sum)])
+    return store(results)
 
 
 def contract_rows(left, right):

time: 99 us -> 92.8 us (0.937)
  other arithmetic: 3.58 us -> 0 us
  local copies, waits for them, and re-layouts: 3.35 us -> 0 us
    add x2 -> x0, other arithmetic: 3.58 us -> none  [the longest x1 2.48 us: fused_body(): up_sum + up_grad]
    unnamed x15 -> x0, local copies, waits for them, and re-layouts: 3.35 us -> none
    pallas_call x0 -> x1, Pallas kernels: none -> 1.88 us  [store(): pl.pallas_call(store_body, out_shape=tuple((jax.ShapeDtypeStruct(r.shape,...]
    pallas_call x1, Pallas kernels: 91.2 us -> 90.1 us  [fused_body(): pl.pallas_call(lambda *refs: fused(a, *refs), out_shape=(jax.ShapeDtypeSt...]
where the time goes in v2:
time: 92.8 us; the launch traced here: 92.6 us
  Pallas kernels  92 us (99%)
    pallas_call x1, Pallas kernels, fused_body(): pl.pallas_call(lambda *refs: fused(a, *refs), out_shape=(jax.ShapeDtypeSt...  90.1 us
    pallas_call x1, Pallas kernels, store(): pl.pallas_call(store_body, out_shape=tuple((jax.ShapeDtypeStruct(r.shape,...  1.88 us

profile of v2, /device:TPU:0, one launch (start us, length us, event | category | flops | bytes accessed | tf_op | source)
XLA Modules:
  0.0 92.6 jit_solution(9871860615636692036)
XLA Ops:
  0.6 90.1 %shard_map.119 = (bf16[128,4096]{1,0:T(8,128)(2,1)S(1)}, bf16[128,1024]{1,0:T(8,128)(2,1)S(1)}, bf16[128,1024]{1,0:T(8,128)(2,1)S(1)}, f32[1024,256]{1,0:T(8,128)S(1)}, f32[256,1024]{1,0:T(8,128)S(1)}) custom-call(bf16[128,1024]{1,0:T(8,128)(2,1)} %refs_0_.1, bf16[1024,256]{1,0:T(8,128)(2,1)} %refs_1_.1, bf16[256,1024]{1,0:T(8,128)(2,1)} %refs_2_.1, ...), custom_call_target="tpu_custom_call" | custom-call | flops 6442450944 | bytes 16777216 | tf_op jit(solution)/shard_map/pallas_call | solution.py:483
  90.8 1.9 %shard_map.120 = (bf16[128,4096]{1,0:T(8,128)(2,1)}, bf16[128,1024]{1,0:T(8,128)(2,1)}, bf16[128,1024]{1,0:T(8,128)(2,1)}, f32[1024,256]{1,0:T(8,128)}, f32[256,1024]{1,0:T(8,128)}) custom-call(bf16[128,4096]{1,0:T(8,128)(2,1)S(1)} %get-tuple-element.10.refs_0_, bf16[128,1024]{1,0:T(8,128)(2,1)S(1)} %get-tuple-element.11.refs_1_, ...), custom_call_target="tpu_custom_call" | custom-call | tf_op jit(solution)/shard_map/pallas_call | solution.py:446

commit v3 on v2

--- a/solution.py
+++ b/solution.py
@@ -1,3 +1,5 @@
+from types import SimpleNamespace
+
 import jax
 import jax.numpy as jnp
 from jax import lax
@@ -196,7 +198,7 @@
             wait(half2(fin_x, 1), 5)
             out[...] = was[...] + (out[...] + (fin_x[...].astype(F32) + fin_y[...].astype(F32)))
 
-        return start, relay, own, finish
+        return SimpleNamespace(start=start, relay=relay, own=own, finish=finish)
 
     def line_sum(which, c, value, staged, from_u, from_d, out):
         own = part.at[which, c]
@@ -244,7 +246,7 @@
 
             out[:, pl.ds(c * cut, cut)] = own[own_rows].astype(BF16)
 
-        return start, relay, finish
+        return SimpleNamespace(start=start, relay=relay, finish=finish)
 
     def hops(b_of, go, offsets=None):
         for o in range(1, a) if offsets is None else offsets:
@@ -256,6 +258,14 @@
     mine = lambda u: t * half_side + u
     other = lambda u: (1 - t) * half_side + u
 
+    def spread(source, target, ss, rs):
+        for k in range(last, 0, -1):
+            for o, cond in ((k, z + k <= last), (a - k, z >= k)):
+                zd = lax.rem(z + o, a)
+                for u in range(half_side):
+                    b = mine(u)
+                    send(source(zd, b), target(b), ss.at[0, o, u], rs.at[0, o, u], (zd * side + q, t), cond)
+
     def pre_relay(o, u, zs, b):
         place = pre_g.at[b, slot(zs)]
         arrive(place, e_ss.at[0, 0, 0], e_rs.at[0, o, u])
@@ -268,9 +278,12 @@
         place = lp_g.at[:, columns(zs * side + b, ff)]
         arrive(place, l_ss.at[0, 0, 0], l_rs.at[0, o, u])
         send(place, place, l_ss.at[1, o, u], l_rs.at[1, o, u], pn)
+        late_pre_o[:, columns(zs * side + b, ff)] = place[...]
 
     def out_rest(o, u, zs, b):
-        arrive(lp_g.at[:, columns(zs * side + b, ff)], l_ss.at[0, 0, 0], l_rs.at[1, o, u])
+        place = lp_g.at[:, columns(zs * side + b, ff)]
+        arrive(place, l_ss.at[0, 0, 0], l_rs.at[1, o, u])
+        late_pre_o[:, columns(zs * side + b, ff)] = place[...]
 
     def ig_value(c):
         return sum(dot(pg[b], up_g[b, pl.ds(c * cut, cut), :], 1, 1) for b in range(side))
@@ -287,145 +300,160 @@
         for c in range(2)
     ]
 
+    def hidden_grad_terms():
+        gather_end("cot")
+        square_rest(1, down_g)
+
+        @pl.loop(0, side)
+        def _(b):
+            gt_s[b] = dot(cot_g[...], down_g[b], 1, 1).astype(BF16)
+
+        send(gt_s, gt_r, t_ss.at[0], t_rs.at[0], pn)
+
+    def early_hidden():
+        for copy in own_pre + own_sums:
+            copy.wait()
+        hops(other, pre_rest)
+
+        @pl.loop(0, side)
+        def _(b):
+            eh[b] = square_relu(pre_g[b])
+
+    def pre_grad():
+        arrive(gt_r, t_ss.at[0], t_rs.at[0])
+
+        @pl.loop(0, side)
+        def _(b):
+            hidden = gt_s[b].astype(F32) + gt_r[b].astype(F32)
+            pg[b] = (hidden * 2.0 * jnp.maximum(pre_g[b].astype(F32), 0.0)).astype(BF16)
+
+    def late_terms():
+        gather_end("late")
+
+        @pl.loop(0, side)
+        def _(b):
+            lt_s[b] = dot(late_g[...], up_g[b], 1, 0).astype(BF16)
+
+        send(lt_s, lt_r, t_ss.at[1], t_rs.at[1], pn)
+
+    def late_hidden():
+        arrive(lt_r, t_ss.at[1], t_rs.at[1])
+
+        @pl.loop(0, side)
+        def _(b):
+            pre = (lt_s[b].astype(F32) + lt_r[b].astype(F32)).astype(BF16)
+            lp[b] = pre
+            lh[b] = square_relu(pre)
+
+    def send_pre():
+        spread(lambda zd, b: early_pre.at[:, columns(zd * side + b, ff)],
+               lambda b: pre_g.at[b, slot(z)], e_ss, e_rs)
+
+    def send_late_pre():
+        spread(lambda zd, b: lp.at[b, slot(zd)],
+               lambda b: lp_g.at[:, columns(z * side + b, ff)], l_ss, l_rs)
+
+    def keep_own():
+        ug[0].own()
+        ug[1].own()
+        for b in range(side):
+            late_pre_o[:, columns(z * side + b, ff)] = lp[b, slot(z)]
+
+    def down_finish():
+        dg.own()
+        dg.finish()
+
+    def relay_rest(name, some=None):
+        for d in range(2, last):
+            gather_relay(name, d, some)
+
+    def own_rest(name):
+        for d in range(2, last):
+            gather_own(name, d)
+
+    def line_rest(chain):
+        chain.relay(2, True)
+        for k in range(3, last):
+            chain.relay(k, False)
+            chain.relay(k, True)
+
     own_down.wait()
     square_send(1, down_g.at[q], down_g)
     own_cot.wait()
     gather_own("cot")
-    for o in range(1, a):
-        zd = lax.rem(z + o, a)
-        for u in range(half_side):
-            b = mine(u)
-            send(early_pre.at[:, columns(zd * side + b, ff)], pre_g.at[b, slot(z)],
-                 e_ss.at[0, o, u], e_rs.at[0, o, u], (zd * side + q, t))
+    gather_relay("cot", 1)
+    square_relay(1, down_g)
+    send_pre()
     own_late.wait()
+    gather_own("late", 1)
+    relay_rest("cot")
+    own_early[0].wait()
+    gather_own("early0", 1)
     gather_own("late", 0)
-    for copy in own_early:
-        copy.wait()
+    own_up.wait()
+    square_send(0, up_g.at[q], up_g)
+    hops(mine, pre_relay, range(3, a))
+    own_rest("late")
+    square_relay(0, up_g)
+    hops(mine, pre_relay, (1,))
     gather_own("early0", 0)
+    gather_relay("late", 1, (0,))
+    gather_relay("late", 1, (1,))
+    hops(mine, pre_relay, (2,))
+    hidden_grad_terms()
+    own_early[1].wait()
     gather_own("early1", 0)
-    own_up.wait()
-    for copy in own_pre:
-        copy.wait()
-    gather_relay("cot", 1)
-    gather_own("late", 1)
-    square_relay(1, down_g)
-    square_send(0, up_g.at[q], up_g)
-    for d in range(2, last):
-        gather_relay("cot", d)
-        gather_own("late", d)
-    hops(mine, pre_relay, (1,))
-    gather_relay("late", 1, (0,))
-    gather_end("cot")
-    square_rest(1, down_g)
-
-    @pl.loop(0, side)
-    def _(b):
-        gt_s[b] = dot(cot_g[...], down_g[b], 1, 1).astype(BF16)
-
-    send(gt_s, gt_r, t_ss.at[0], t_rs.at[0], pn)
-    square_relay(0, up_g)
-    hops(mine, pre_relay, range(2, a))
-    gather_relay("late", 1, (1,))
-    gather_own("early0", 1)
     gather_own("early1", 1)
-    hops(other, pre_rest)
-
-    @pl.loop(0, side)
-    def _(b):
-        eh[b] = square_relu(pre_g[b])
-
-    arrive(gt_r, t_ss.at[0], t_rs.at[0])
-
-    @pl.loop(0, side)
-    def _(b):
-        hidden = gt_s[b].astype(F32) + gt_r[b].astype(F32)
-        pg[b] = (hidden * 2.0 * jnp.maximum(pre_g[b].astype(F32), 0.0)).astype(BF16)
-
-    dg_start, dg_relay, dg_own, dg_finish = dg
-    dg_start()
+    early_hidden()
+    pre_grad()
     gather_relay("early0", 1)
+    dg.start()
+    relay_rest("late", (0,))
+    relay_rest("late", (1,))
     square_rest(0, up_g)
-    ig[0][0]()
-    gather_relay("late", 2, (0,))
-    ig[1][0]()
-    dg_relay()
-    gather_relay("late", 2, (1,))
-    for d in range(3, last):
-        gather_relay("late", d)
-    for d in range(2, last):
-        gather_own("early0", d)
-        gather_own("early1", d)
+    ig[0].start()
     gather_relay("early1", 1)
-    ig[0][1](1, True)
-    gather_end("late")
-
-    @pl.loop(0, side)
-    def _(b):
-        lt_s[b] = dot(late_g[...], up_g[b], 1, 0).astype(BF16)
-
-    send(lt_s, lt_r, t_ss.at[1], t_rs.at[1], pn)
-    ig[0][1](2, False)
-    for d in range(2, last):
-        gather_relay("early0", d)
-    arrive(lt_r, t_ss.at[1], t_rs.at[1])
-
-    @pl.loop(0, side)
-    def _(b):
-        pre = (lt_s[b].astype(F32) + lt_r[b].astype(F32)).astype(BF16)
-        lp[b] = pre
-        lh[b] = square_relu(pre)
-
-    lo[0][0]()
-    lo[1][0]()
-    for o in range(1, a):
-        zd = lax.rem(z + o, a)
-        for u in range(half_side):
-            b = mine(u)
-            send(lp.at[b, slot(zd)], lp_g.at[:, columns(z * side + b, ff)],
-                 l_ss.at[0, o, u], l_rs.at[0, o, u], (zd * side + q, t))
-    ig[1][1](1, True)
-    for d in range(2, last):
-        gather_relay("early1", d)
+    own_rest("early0")
+    ig[1].start()
+    ig[0].relay(1, True)
+    own_rest("early1")
+    relay_rest("early0")
+    late_terms()
+    ig[0].relay(2, False)
+    late_hidden()
+    ig[1].relay(1, True)
+    relay_rest("early1")
+    lo[0].start()
+    dg.relay()
+    lo[1].start()
+    ig[1].relay(2, False)
     gather_end("early0")
-    ug[0][0]()
-    ig[1][1](2, False)
-    ig[0][1](2, True)
-    lo[0][1](1, True)
-    dg_own()
-    for copy in own_sums:
-        copy.wait()
-    dg_finish()
-    ug[0][1]()
-    ig[1][1](2, True)
-    for k in range(3, last):
-        for c in range(2):
-            for opening in (False, True):
-                ig[c][1](k, opening)
+    ug[0].start()
     gather_end("early1")
-    ug[1][0]()
-    lo[0][1](2, False)
-    lo[0][1](2, True)
-    lo[1][1](1, True)
-    ug[1][1]()
-    ig[0][2]()
-    ig[1][2]()
-    lo[1][1](2, False)
-    lo[1][1](2, True)
-    for k in range(3, last):
-        for c in range(2):
-            for opening in (False, True):
-                lo[c][1](k, opening)
-    for b in range(side):
-        lp_g[:, columns(z * side + b, ff)] = lp[b, slot(z)]
-    ug[0][2]()
-    ug[1][2]()
-    hops(mine, out_relay)
-    ug[0][3]()
-    lo[0][2]()
-    ug[1][3]()
-    lo[1][2]()
+    ug[1].start()
+    send_late_pre()
+    line_rest(ig[0])
+    lo[0].relay(1, True)
+    keep_own()
+    lo[1].relay(1, True)
+    line_rest(ig[1])
+    lo[0].relay(2, False)
+    ug[0].relay()
+    ig[1].finish()
+    ug[1].relay()
+    line_rest(lo[0])
+    ug[0].finish()
+    ig[0].finish()
+    lo[1].relay(2, False)
+    line_rest(lo[1])
+    down_finish()
+    lo[0].finish()
+    hops(mine, out_relay, (2,))
+    hops(mine, out_relay, range(3, a))
+    hops(mine, out_relay, (1,))
+    ug[1].finish()
+    lo[1].finish()
     hops(other, out_rest)
-    late_pre_o[...] = lp_g[...]
 
     for cond, copy in sent:
         run(cond, copy.wait_send)

time: 92.8 us -> 90.6 us (0.976)
  Pallas kernels: 92 us -> 89.8 us
    pallas_call x1, Pallas kernels: 90.1 us -> 87.9 us  [fused_body(): pl.pallas_call(lambda *refs: fused(a, *refs), out_shape=(jax.ShapeDtypeSt...]
where the time goes in v3:
time: 90.6 us; the launch traced here: 90.5 us
  Pallas kernels  89.8 us (99%)
    pallas_call x1, Pallas kernels, fused_body(): pl.pallas_call(lambda *refs: fused(a, *refs), out_shape=(jax.ShapeDtypeSt...  87.9 us
    pallas_call x1, Pallas kernels, store(): pl.pallas_call(store_body, out_shape=tuple((jax.ShapeDtypeStruct(r.shape,...  1.88 us

profile of v3, /device:TPU:0, one launch (start us, length us, event | category | flops | bytes accessed | tf_op | source)
XLA Modules:
  0.0 90.5 jit_solution(7602621698714596386)
XLA Ops:
  0.6 87.9 %shard_map.119 = (bf16[128,4096]{1,0:T(8,128)(2,1)S(1)}, bf16[128,1024]{1,0:T(8,128)(2,1)S(1)}, bf16[128,1024]{1,0:T(8,128)(2,1)S(1)}, f32[1024,256]{1,0:T(8,128)S(1)}, f32[256,1024]{1,0:T(8,128)S(1)}) custom-call(bf16[128,1024]{1,0:T(8,128)(2,1)} %refs_0_.1, bf16[1024,256]{1,0:T(8,128)(2,1)} %refs_1_.1, bf16[256,1024]{1,0:T(8,128)(2,1)} %refs_2_.1, ...), custom_call_target="tpu_custom_call" | custom-call | flops 6442450944 | bytes 16777216 | tf_op jit(solution)/shard_map/pallas_call | solution.py:511
  88.6 1.9 %shard_map.120 = (bf16[128,4096]{1,0:T(8,128)(2,1)}, bf16[128,1024]{1,0:T(8,128)(2,1)}, bf16[128,1024]{1,0:T(8,128)(2,1)}, f32[1024,256]{1,0:T(8,128)}, f32[256,1024]{1,0:T(8,128)}) custom-call(bf16[128,4096]{1,0:T(8,128)(2,1)S(1)} %get-tuple-element.10.refs_0_, bf16[128,1024]{1,0:T(8,128)(2,1)S(1)} %get-tuple-element.11.refs_1_, ...), custom_call_target="tpu_custom_call" | custom-call | tf_op jit(solution)/shard_map/pallas_call | solution.py:474

commit v4 on v3

--- a/solution.py
+++ b/solution.py
@@ -27,7 +27,7 @@
           part, ig_s, ig_u, ig_d, lo_s, lo_u, lo_d,
           dg_s, dg_x, dg_y, dg_fx, dg_fy, ug_s, ug_x, ug_y, ug_fx, ug_fy,
           ag_ss, ag_rs, w_ss, w_rs, e_ss, e_rs, l_ss, l_rs, t_ss, t_rs, rl_ss, rl_rs, rq_ss, rq_rs,
-          local_s, up_was, down_was):
+          local_s, up_was, down_was, line_s):
     side = 4
     half_side = side // 2
     me = lax.axis_index("fs")
@@ -67,8 +67,8 @@
         return pl.ds(pl.multiple_of(block * unit, unit), unit)
 
     own_rows = slot(z)
+    own_cot = begin(cot, cot_g.at[own_rows], 1)
     own_down = begin(down_w, down_g.at[q], 0)
-    own_cot = begin(cot, cot_g.at[own_rows], 1)
     own_late = begin(late_in, late_g.at[own_rows], 3)
     own_early = [begin(early_in.at[:, pl.ds(c * cut, cut)], early_g.at[c, own_rows], 9 + c) for c in range(2)]
     own_up = begin(up_w, up_g.at[q], 2)
@@ -78,13 +78,25 @@
         for b in range(side)
     ]
 
-    own_sums = [begin(up_old, up_was, 11), begin(down_old, down_was, 12)]
 
     barrier = pltpu.get_barrier_semaphore()
-    greet = [xn, yn, pn] + [(lax.rem(me + o * side, a * side), t) for o in range(1, a)]
-    for device in greet:
-        pl.semaphore_signal(barrier, inc=1, device_id=device, device_id_type=MESH)
-    pl.semaphore_wait(barrier, len(greet))
+    has_above = z < last
+    has_below = z > 0
+
+    def signal(semaphore, device):
+        pl.semaphore_signal(semaphore, inc=1, device_id=device, device_id_type=MESH)
+
+    for device in (xn, yn, pn):
+        signal(barrier, device)
+    pl.when(has_above)(lambda: signal(barrier, above))
+    pl.when(has_below)(lambda: signal(barrier, below))
+    pl.semaphore_wait(barrier, 3 + jnp.where(has_above, 1, 0) + jnp.where(has_below, 1, 0))
+
+    def line_entered():
+        pl.when(has_above)(lambda: pl.semaphore_wait(line_s.at[0], 1))
+        pl.when(has_below)(lambda: signal(line_s.at[0], below))
+        pl.when(has_below)(lambda: pl.semaphore_wait(line_s.at[1], 1))
+        pl.when(has_above)(lambda: signal(line_s.at[1], above))
 
     sent = []
 
@@ -102,6 +114,11 @@
         copy = rc(src, dst, ss, rs, device)
         run(cond, copy.start)
         sent.append((cond, copy))
+
+    def settle(count):
+        for cond, copy in sent[:count]:
+            run(cond, copy.wait_send)
+        del sent[:count]
 
     def arrive(dst, ss, rs, cond=None):
         run(cond, rc(dst, dst, ss, rs, pn).wait_recv)
@@ -377,10 +394,12 @@
             chain.relay(k, False)
             chain.relay(k, True)
 
+    own_cot.wait()
+    gather_own("cot")
     own_down.wait()
     square_send(1, down_g.at[q], down_g)
-    own_cot.wait()
-    gather_own("cot")
+    own_sums = [begin(up_old, up_was, 11), begin(down_old, down_was, 12)]
+    line_entered()
     gather_relay("cot", 1)
     square_relay(1, down_g)
     send_pre()
@@ -421,6 +440,7 @@
     late_terms()
     ig[0].relay(2, False)
     late_hidden()
+    settled = len(sent)
     ig[1].relay(1, True)
     relay_rest("early1")
     lo[0].start()
@@ -448,6 +468,7 @@
     line_rest(lo[1])
     down_finish()
     lo[0].finish()
+    settle(settled)
     hops(mine, out_relay, (2,))
     hops(mine, out_relay, range(3, a))
     hops(mine, out_relay, (1,))
@@ -455,8 +476,7 @@
     lo[1].finish()
     hops(other, out_rest)
 
-    for cond, copy in sent:
-        run(cond, copy.wait_send)
+    settle(len(sent))
 
 
 def store_body(*refs):
@@ -505,7 +525,7 @@
         + [D((6, 2, a)), D((6, 2, a)), D((2, 2, 3)), D((2, 2, 3)), D((2, a, 2)), D((2, a, 2)),
            D((2, a, 2)), D((2, a, 2)), D((2,)), D((2,)), D((2, 2, 2, a)), D((2, 2, 2, a)),
            D((2, 2, 6)), D((2, 2, 6)), D((13,))]
-        + [V((width, ff), F32), V((ff, width), F32)]
+        + [V((width, ff), F32), V((ff, width), F32), pltpu.SemaphoreType.REGULAR((2,))]
     )
     flops = 12 * tokens * hidden * width
     results = pl.pallas_call(

time: 90.6 us -> 90.2 us (level); the launches traced: 90.5 us -> 89.1 us
  Pallas kernels: 89.8 us -> 88.5 us
    pallas_call x1, Pallas kernels: 87.9 us -> 86.6 us  [fused_body(): pl.pallas_call(lambda *refs: fused(a, *refs), out_shape=(jax.ShapeDtypeSt...]
where the time goes in v4:
time: 90.2 us; the launch traced here: 89.1 us
  Pallas kernels  88.5 us (98%)
    pallas_call x1, Pallas kernels, fused_body(): pl.pallas_call(lambda *refs: fused(a, *refs), out_shape=(jax.ShapeDtypeSt...  86.6 us
    pallas_call x1, Pallas kernels, store(): pl.pallas_call(store_body, out_shape=tuple((jax.ShapeDtypeStruct(r.shape,...  1.88 us

profile of v4, /device:TPU:0, one launch (start us, length us, event | category | flops | bytes accessed | tf_op | source)
XLA Modules:
  0.0 89.1 jit_solution(15774400738317901504)
XLA Ops:
  0.6 86.6 %shard_map.119 = (bf16[128,4096]{1,0:T(8,128)(2,1)S(1)}, bf16[128,1024]{1,0:T(8,128)(2,1)S(1)}, bf16[128,1024]{1,0:T(8,128)(2,1)S(1)}, f32[1024,256]{1,0:T(8,128)S(1)}, f32[256,1024]{1,0:T(8,128)S(1)}) custom-call(bf16[128,1024]{1,0:T(8,128)(2,1)} %refs_0_.1, bf16[1024,256]{1,0:T(8,128)(2,1)} %refs_1_.1, bf16[256,1024]{1,0:T(8,128)(2,1)} %refs_2_.1, ...), custom_call_target="tpu_custom_call" | custom-call | flops 6442450944 | bytes 16777216 | tf_op jit(solution)/shard_map/pallas_call | solution.py:531
  87.2 1.9 %shard_map.120 = (bf16[128,4096]{1,0:T(8,128)(2,1)}, bf16[128,1024]{1,0:T(8,128)(2,1)}, bf16[128,1024]{1,0:T(8,128)(2,1)}, f32[1024,256]{1,0:T(8,128)}, f32[256,1024]{1,0:T(8,128)}) custom-call(bf16[128,4096]{1,0:T(8,128)(2,1)S(1)} %get-tuple-element.10.refs_0_, bf16[128,1024]{1,0:T(8,128)(2,1)S(1)} %get-tuple-element.11.refs_1_, ...), custom_call_target="tpu_custom_call" | custom-call | tf_op jit(solution)/shard_map/pallas_call | solution.py:494

commit v5 on v4

--- a/solution.py
+++ b/solution.py
@@ -472,6 +472,7 @@
     hops(mine, out_relay, (2,))
     hops(mine, out_relay, range(3, a))
     hops(mine, out_relay, (1,))
+    settle(len(sent))
     ug[1].finish()
     lo[1].finish()
     hops(other, out_rest)

time: 90.2 us -> 90.1 us (level)
  no operation moved by 1% of the time
where the time goes in v5:
time: 90.1 us; the launch traced here: 89 us
  Pallas kernels  88.4 us (98%)
    pallas_call x1, Pallas kernels, fused_body(): pl.pallas_call(lambda *refs: fused(a, *refs), out_shape=(jax.ShapeDtypeSt...  86.5 us
    pallas_call x1, Pallas kernels, store(): pl.pallas_call(store_body, out_shape=tuple((jax.ShapeDtypeStruct(r.shape,...  1.88 us

profile of v5, /device:TPU:0, one launch (start us, length us, event | category | flops | bytes accessed | tf_op | source)
XLA Modules:
  0.0 89.0 jit_solution(7139758314666963512)
XLA Ops:
  0.6 86.5 %shard_map.119 = (bf16[128,4096]{1,0:T(8,128)(2,1)S(1)}, bf16[128,1024]{1,0:T(8,128)(2,1)S(1)}, bf16[128,1024]{1,0:T(8,128)(2,1)S(1)}, f32[1024,256]{1,0:T(8,128)S(1)}, f32[256,1024]{1,0:T(8,128)S(1)}) custom-call(bf16[128,1024]{1,0:T(8,128)(2,1)} %refs_0_.1, bf16[1024,256]{1,0:T(8,128)(2,1)} %refs_1_.1, bf16[256,1024]{1,0:T(8,128)(2,1)} %refs_2_.1, ...), custom_call_target="tpu_custom_call" | custom-call | flops 6442450944 | bytes 16777216 | tf_op jit(solution)/shard_map/pallas_call | solution.py:532
  87.1 1.9 %shard_map.120 = (bf16[128,4096]{1,0:T(8,128)(2,1)}, bf16[128,1024]{1,0:T(8,128)(2,1)}, bf16[128,1024]{1,0:T(8,128)(2,1)}, f32[1024,256]{1,0:T(8,128)}, f32[256,1024]{1,0:T(8,128)}) custom-call(bf16[128,4096]{1,0:T(8,128)(2,1)S(1)} %get-tuple-element.10.refs_0_, bf16[128,1024]{1,0:T(8,128)(2,1)S(1)} %get-tuple-element.11.refs_1_, ...), custom_call_target="tpu_custom_call" | custom-call | tf_op jit(solution)/shard_map/pallas_call | solution.py:495
